TPU v7x, 32 devices: a whole 2x2x4 slice. The times are simulated.
32 devices in a mesh: ep: 8 (over z, x), tp: 4 (over y, core).
Axes of the slice: x: 2, y: 2, z: 4, core: 2. Of those that a mesh axis runs over, the one named last changes fastest.
Arguments:
- x_in: bfloat16 [4096, 3072], P('tp', 'ep'), may hold values from -6 to 6
- z_in: bfloat16 [4096, 3072], P('tp', 'ep'), may hold values from -6 to 6
- dt_raw: float32 [64, 3072], P('tp', 'ep'), may hold values from -6 to 6
- decay_rate: float32 [64], P('tp'), may hold values from 0 to 1, as said below
- b_in: bfloat16 [256, 3072], P(None, 'ep'), may hold values from -6 to 6
- c_in: bfloat16 [256, 3072], P(None, 'ep'), may hold values from -6 to 6
- conv_x: float32 [4096, 4], P('tp'), may hold values from -3 to 3
- conv_b: float32 [256, 4], replicated, may hold values from -3 to 3
- conv_c: float32 [256, 4], replicated, may hold values from -3 to 3
- head_gain: float32 [4096], P('tp'), may hold values from 0.1 to 1.9
- moe_rows: bfloat16 [1280, 2048], P('ep'), may hold values from -6 to 6
- moe_gain: float32 [2048], replicated, may hold values from 0.1 to 1.9
- routes: int32 [1280, 2], P('ep'), may hold values from 0 to 7, all different within a row; in each aligned block of 160 rows (0 to 159, 160 to 319, ...) at most 80 rows name the same one
- route_logit: float32 [1280, 2], P('ep'), may hold values from -6 to 6
- w_gate: bfloat16 [8, 2048, 5120], P('ep', None, 'tp'), may hold values from -0.125 to 0.125
- w_up: bfloat16 [8, 2048, 5120], P('ep', None, 'tp'), may hold values from -0.125 to 0.125
- w_down: bfloat16 [8, 5120, 2048], P('ep', 'tp'), may hold values from -0.078125 to 0.078125
Outputs:
- mixed: bfloat16 [4096, 3072], P('tp', 'ep')
- moe_out: bfloat16 [2048, 1280], P('tp', 'ep')
Inputs may be any that keep to these rules, and one draw needn't show every extreme that they name: `routes`: each row names 2 different experts; among the rows of one index of ep no expert is named more than 80 times, a bound that some block reaches. `decay_rate`: positive rates.
All inputs are finite; a program needn't handle non-finite values.
Results may differ from a plain program's by a relative error of at most 0.018.
Values may be sent and summed in bfloat16 or wider, within the bound.
No kernel may reach another device: no remote copies, remote signals or barrier semaphores. Data moves between devices by JAX's collectives and lax.ppermute only.
A program may use at most 64 MiB of HBM per device.

v0:
```python
import jax
import jax.numpy as jnp
from jax import lax
from jax.sharding import PartitionSpec as P

HEADS = 64
HEAD_DIM = 64
GROUPS = 2
NSTATE = 128
BLOCK = 128
EXP_DEV = 1
HIGHEST = lax.Precision.HIGHEST
ROW_EPS = 0.1
HEAD_EPS = 1.0


def from_behind(value, axis, steps):
    count = lax.axis_size(axis)
    initial, last = (max(0, -steps), min(count, count - steps))
    return lax.ppermute(value, axis, [(source, source + steps) for source in range(initial, last)])


def carried_in(shard, axis, join, neutral):
    place = lax.axis_index(axis)
    gathered = jax.tree.map(
        lambda a, kind: lax.all_gather(a.astype(kind), axis), shard, (jnp.bfloat16, jnp.bfloat16)
    )
    state = jax.tree.map(lambda a, e: jnp.zeros_like(a) + jnp.asarray(e, a.dtype), shard, neutral)

    def one(turn, state):
        return join(
            state,
            jax.tree.map(
                lambda a, own: lax.dynamic_index_in_dim(a, turn, 0, False).astype(own.dtype),
                gathered,
                shard,
            ),
        )

    return lax.fori_loop(0, place, one, state)


def conv_with_rims(signal, rim_rows, weight):
    taps = weight.shape[1]
    length = signal.shape[1]
    joined = jnp.concatenate([rim_rows.astype(jnp.float32), signal.astype(jnp.float32)], axis=1)
    running = jnp.zeros(signal.shape, jnp.float32)
    for offset in range(taps):
        running = running + weight[:, offset : offset + 1] * joined[:, offset : offset + length]
    return jax.nn.silu(running)


def block_step(state_in, x_block, b_block, c_block, log_block, step_block):
    cum_log = jnp.cumsum(log_block, axis=1)
    seg_log = cum_log[:, :, None] - cum_log[:, None, :]
    causal = jnp.tril(jnp.ones((log_block.shape[1], log_block.shape[1]), bool))
    decay_mask = jnp.exp(jnp.where(causal[None], seg_log, -jnp.inf))
    scores = (
        jnp.einsum("hnt,hns->hts", c_block, b_block, precision=HIGHEST)
        * decay_mask
        * step_block[:, None, :]
    )
    inner_term = jnp.einsum("hts,hps->hpt", scores, x_block, precision=HIGHEST)
    carried = (
        jnp.einsum("hnt,hpn->hpt", c_block, state_in, precision=HIGHEST)
        * jnp.exp(cum_log)[:, None, :]
    )
    tail_weight = jnp.exp(cum_log[:, -1:] - cum_log) * step_block
    fresh_state = jnp.einsum(
        "hps,hns->hpn", x_block * tail_weight[:, None, :], b_block, precision=HIGHEST
    )
    new_state = jnp.exp(cum_log[:, -1])[:, None, None] * state_in + fresh_state
    return (new_state, inner_term + carried)


def combine_states(before_part, after_part):
    return (
        before_part[0] * after_part[0],
        after_part[0][..., None, None] * before_part[1] + after_part[1],
    )


def mixer_half(x_in, z_in, dt_raw, decay_rate, b_in, c_in, conv_x, conv_b, conv_c, head_gain):
    head_count = dt_raw.shape[0]
    length = dt_raw.shape[1]
    taps = conv_x.shape[1]
    value_rows = x_in.shape[0]
    per_group = HEADS // GROUPS
    group_index = lax.axis_index("tp") * head_count // per_group
    b_own = lax.dynamic_slice_in_dim(b_in, group_index * NSTATE, NSTATE, 0)
    c_own = lax.dynamic_slice_in_dim(c_in, group_index * NSTATE, NSTATE, 0)
    taps_b = lax.dynamic_slice_in_dim(conv_b, group_index * NSTATE, NSTATE, 0)
    taps_c = lax.dynamic_slice_in_dim(conv_c, group_index * NSTATE, NSTATE, 0)
    edge = length - taps + 1
    own_rims = jnp.concatenate([x_in[:, edge:], b_own[:, edge:], c_own[:, edge:]], axis=0)
    rims = from_behind(own_rims, "ep", 1)
    x_conv = conv_with_rims(x_in, rims[:value_rows], conv_x).reshape(head_count, HEAD_DIM, length)
    b_conv = conv_with_rims(b_own, rims[value_rows : value_rows + NSTATE], taps_b)
    c_conv = conv_with_rims(c_own, rims[value_rows + NSTATE :], taps_c)
    step_dt = jax.nn.softplus(dt_raw)
    log_decay = -step_dt * decay_rate[:, None]
    block_count = length // BLOCK

    def blocks(tensor):
        return jnp.moveaxis(tensor.reshape(tensor.shape[:-1] + (block_count, BLOCK)), -2, 0)

    def spread_heads(tensor):
        return jnp.broadcast_to(tensor[None], (head_count,) + tensor.shape)

    def advance(state_in, inputs):
        x_block, b_block, c_block, log_block, step_block = inputs
        return block_step(
            state_in, x_block, spread_heads(b_block), spread_heads(c_block), log_block, step_block
        )

    init_state = jnp.zeros((head_count, HEAD_DIM, NSTATE), jnp.float32)
    local_state, block_out = lax.scan(
        advance,
        init_state,
        (blocks(x_conv), blocks(b_conv), blocks(c_conv), blocks(log_decay), blocks(step_dt)),
    )
    y_local = jnp.moveaxis(block_out, 0, -2).reshape(head_count, HEAD_DIM, length)
    total_decay = jnp.exp(jnp.sum(log_decay, axis=1))
    _, incoming = carried_in(
        (total_decay, local_state),
        "ep",
        combine_states,
        (jnp.ones_like(total_decay), jnp.zeros_like(local_state)),
    )
    reach_decay = jnp.exp(jnp.cumsum(log_decay, axis=1))
    carried = (
        jnp.einsum("nt,hpn->hpt", c_conv, incoming, precision=HIGHEST) * reach_decay[:, None, :]
    )
    y_mixed = y_local + carried
    gated_out = y_mixed * jax.nn.silu(
        z_in.astype(jnp.float32).reshape(head_count, HEAD_DIM, length)
    )
    head_scale = lax.rsqrt(jnp.mean(gated_out * gated_out, axis=1, keepdims=True) + HEAD_EPS)
    normed_out = gated_out * head_scale * head_gain.reshape(head_count, HEAD_DIM, 1)
    return normed_out.reshape(head_count * HEAD_DIM, length).astype(jnp.bfloat16)


def experts_half(moe_rows, moe_gain, routes, route_logit, w_gate, w_up, w_down):
    tokens = moe_rows.shape[0]
    top_count = routes.shape[1]
    features = moe_gain.shape[0]
    experts = EXP_DEV * lax.axis_size("ep")
    capacity = 2 * tokens * top_count // experts
    col_width = features // lax.axis_size("tp")
    rows_float = moe_rows.astype(jnp.float32)
    row_scale = lax.rsqrt(jnp.mean(rows_float * rows_float, axis=1, keepdims=True) + ROW_EPS)
    normed_float = rows_float * row_scale * moe_gain
    flat_routes = routes.reshape(-1)
    hit_table = (flat_routes[:, None] == jnp.arange(experts, dtype=jnp.int32)[None, :]).astype(
        jnp.int32
    )
    slot_rank = jnp.sum((jnp.cumsum(hit_table, axis=0) - hit_table) * hit_table, axis=1)
    slot_index = flat_routes * capacity + slot_rank
    owner_row = jnp.arange(tokens * top_count, dtype=jnp.int32) // top_count
    column = lax.axis_index("tp") * col_width
    normed = lax.dynamic_slice_in_dim(normed_float.astype(jnp.bfloat16), column, col_width, 1)
    outbox = (
        jnp.zeros((experts * capacity, col_width), jnp.bfloat16)
        .at[slot_index]
        .set(normed[owner_row])
    )
    arrived = lax.all_to_all(
        outbox.reshape(experts, capacity, col_width), "ep", split_axis=0, concat_axis=0, tiled=True
    ).reshape(-1, col_width)
    part_rows = lax.all_gather(arrived, "tp", axis=1, tiled=True)
    gate_rows = w_gate[0]
    up_rows = w_up[0]
    gate_act = jnp.dot(part_rows, gate_rows, preferred_element_type=jnp.float32)
    up_act = jnp.dot(part_rows, up_rows, preferred_element_type=jnp.float32)
    hidden = (jax.nn.silu(gate_act) * up_act).astype(jnp.bfloat16)
    columns = w_down[0]
    summed = lax.psum_scatter(
        lax.dot_general(
            columns, hidden, (((0,), (1,)), ((), ())), preferred_element_type=jnp.float32
        ).astype(jnp.bfloat16),
        "tp",
        scatter_dimension=0,
        tiled=True,
    )
    expert_out = summed.reshape(col_width, experts, capacity)
    returned = lax.all_to_all(expert_out, "ep", split_axis=1, concat_axis=1, tiled=True)
    picked = returned.reshape(col_width, experts * capacity)[:, slot_index].astype(jnp.float32)
    picked = picked.reshape(col_width, tokens, top_count)
    weight = jax.nn.sigmoid(route_logit - route_logit[:, ::-1])
    combined = jnp.sum(picked * weight[None], axis=2)
    return combined.astype(jnp.bfloat16)


def on_device(
    x_in,
    z_in,
    dt_raw,
    decay_rate,
    b_in,
    c_in,
    conv_x,
    conv_b,
    conv_c,
    head_gain,
    moe_rows,
    moe_gain,
    routes,
    route_logit,
    w_gate,
    w_up,
    w_down,
):
    mixed = mixer_half(
        x_in, z_in, dt_raw, decay_rate, b_in, c_in, conv_x, conv_b, conv_c, head_gain
    )
    moe_out = experts_half(moe_rows, moe_gain, routes, route_logit, w_gate, w_up, w_down)
    return (mixed, moe_out)


def solution(mesh):
    return jax.shard_map(
        on_device,
        mesh=mesh,
        in_specs=(
            P("tp", "ep"),
            P("tp", "ep"),
            P("tp", "ep"),
            P("tp"),
            P(None, "ep"),
            P(None, "ep"),
            P("tp", None),
            P(),
            P(),
            P("tp"),
            P("ep", None),
            P(),
            P("ep", None),
            P("ep", None),
            P("ep", None, "tp"),
            P("ep", None, "tp"),
            P("ep", "tp", None),
        ),
        out_specs=(P("tp", "ep"), P("tp", "ep")),
        check_vma=False,
    )
```

profile of v0, /device:TPU:31, one launch (start us, length us, event | category | flops | bytes accessed | tf_op | source)
XLA Modules:
  0.0 211.8 jit_solution(18337351531180557523)
XLA Ops:
  12.3 3.4 %scatter_custom_fusion = bf16[640,512]{1,0:T(8,128)(2,1)S(1)} fusion(s32[320]{0:T(512)S(1)} %get-tuple-element.186, bf16[160,512]{1,0:T(8,128)(2,1)S(1)} %fusion.45, s32[1024]{0:T(1024)S(1)} %pad_clamp_fusion.1, bf16[]{:T(256)} %constant.124.clone.1), kind=kCustom, calls=%fused_computation.70 | custom fusion | bytes 655362 | tf_op jit(solution)/shard_map/scatter | solution.py:165
  15.8 20.8 %all_to_all.10 = bf16[8,80,512]{2,1,0:T(8,128)(2,1)} all-to-all(bf16[8,80,512]{2,1,0:T(8,128)(2,1)S(1)} %bitcast.153), channel_id=1, replica_groups=mesh['ep'=8,'tp'=4] {'ep'}, dimensions={0} | all-to-all | bytes 1310720 | tf_op jit(solution)/shard_map/all_to_all | solution.py:167
  37.3 1.5 collective-permute-start
  42.0 3.2 %divide_multiply_fusion = f32[1024,384]{1,0:T(8,128)} fusion(f32[1024,384]{1,0:T(8,128)S(1)} %convert_element_type.89, f32[1024,3]{1,0:T(8,128)S(1)} %copy.41, f32[1024]{0:T(1024)S(1)} %bitcast.164, f32[1024]{0:T(1024)S(1)} %bitcast.165, f32[1024]{0:T(1024)S(1)} %bitcast.163, f32[1024]{0:T(1024)S(1)} %bitcast.162), kind=kLoop, calls=%fused_computation.63 | loop fusion | flops 5505024 | bytes 3174400 | tf_op jit(solution)/shard_map/jit(silu)/mul | solution.py:50
  45.2 2.6 %reshape_reshape.3 = f32[16,64,3,128]{3,2,1,0:T(4,128)S(1)} reshape(f32[1024,384]{1,0:T(8,128)} %divide_multiply_fusion) | data formatting | bytes 3145728 | tf_op jit(solution)/shard_map/reshape;reshape | solution.py:105
  48.1 14.7 %all-gather.5.cloned.1.call-done = bf16[640,2048]{1,0:T(8,128)(2,1)} async-done(((bf16[640,512]{1,0:T(8,128)(2,1)}), bf16[640,2048]{1,0:T(8,128)(2,1)}) %all-gather.5.cloned.1.call-update) | async-done | bytes 2621456 | tf_op jit(solution)/shard_map/all_gather | solution.py:170
  62.8 8.5 %fusion.18 = f32[640,1280]{1,0:T(8,128)} fusion(bf16[640,2048]{1,0:T(8,128)(2,1)} %all-gather.5.cloned.1.call-done, bf16[1,2048,1280]{2,1,0:T(8,128)(2,1)} %param.35), kind=kOutput, calls=%fused_computation.35 | convolution fusion | flops 3355443200 | bytes 11141120 | tf_op jit(solution)/shard_map/dot_general | solution.py:173
  71.3 15.2 %fusion.29 = bf16[2048,640]{0,1:T(8,128)(2,1)} fusion(bf16[1,1280,2048]{2,1,0:T(8,128)(2,1)} %param.37, bf16[640,2048]{1,0:T(8,128)(2,1)} %all-gather.5.cloned.1.call-done, bf16[1,2048,1280]{2,1,0:T(8,128)(2,1)} %param.36, f32[640,1280]{1,0:T(8,128)} %fusion.18), kind=kOutput, calls=%fused_computation.40 | convolution fusion | flops 6717112320 | bytes 19005440 | tf_op jit(solution)/shard_map/dot_general | solution.py:178
  86.8 40.6 %while.26 = (s32[]{:T(128)}, f32[16,64,128]{2,1,0:T(8,128)S(1)}, f32[3,16,64,128]{3,2,1,0:T(8,128)}, f32[3,16,128]{2,0,1:T(4,128)S(1)}, f32[3,16,64,128]{3,0,2,1...) while((s32[]{:T(128)}, f32[16,64,128]{2,1,0:T(8,128)S(1)}, ...), condition=%wide.region_2.3_spmd.clone, body=%wide.region_0.2_spmd.clone.sunk | while | flops 1008879616 | bytes 10045104 | solution.py:117
  86.8 1.4 constant_dynamic-slice_fusion.14
  90.1 1.6 fusion.104
  91.9 2.7 %fusion.105 = f32[16,128,128]{2,1,0:T(8,128)S(1)} fusion(f32[16,128]{1,0:T(8,128)} %bitcast.142, f32[16,128]{1,0:T(8,128)S(1)} %reduce_window_sum.51, f32[128,128]{1,0:T(8,128)S(1)} %bitcast.151, f32[128,128]{1,0:T(8,128)S(1)} %bitcast.148, pred[128,128]{1,0:T(8,128)(4,1)S(1)} %iota_compare_fusion.4), kind=kOutput, calls=%fused_computation.6.clone.1 | convolution fusion | flops 403701760 | bytes 1212416 | tf_op jit(solution)/shard_map/while/body/eval_jaxpr/hnt,hns->hts/dot_general | solution.py:59
  95.2 3.0 %fusion.106 = f32[3,16,64,128]{3,2,1,0:T(8,128)} fusion(f32[3,16,64,128]{3,2,1,0:T(8,128)} %get-tuple-element.298, s32[]{:T(128)} %get-tuple-element.296, f32[16,64,128]{2,1,0:T(8,128)S(1)} %fusion.104, f32[16,64,128]{2,1,0:T(8,128)S(1)} %bitcast.144, f32[16,128,128]{2,1,0:T(8,128)S(1)} %fusion.105), kind=kOutput, calls=%fused_computation.11.clone.1 | convolution fusion | flops 201457664 | bytes 2621952 | tf_op jit(solution)/shard_map/while/body/eval_jaxpr/hts,hps->hpt/dot_general | solution.py:63
  98.2 2.1 %convolution_add_fusion.3 = f32[16,64,128]{2,1,0:T(8,128)S(1)} fusion(f32[128,128]{1,0:T(8,128)S(1)} %bitcast.149, f32[16,64,128]{2,1,0:T(8,128)S(1)} %bitcast.145, f32[16,64,128]{2,1,0:T(8,128)S(1)} %get-tuple-element.297, f32[16,128]{1,0:T(8,128)S(1)} %get-tuple-element.282, f32[16]{0:T(128)S(1)} %exp.118, pred[]{:T(512)S(6)} %compare.10), kind=kOutput, calls=%fused_computation.12.clone.1 | convolution fusion | flops 201850880 | bytes 1646657 | tf_op jit(solution)/shard_map/while/body/eval_jaxpr/hps,hns->hpn/dot_general | solution.py:69
  100.4 1.4 constant_dynamic-slice_fusion.14
  103.7 1.6 fusion.104
  105.5 2.7 %fusion.105 = f32[16,128,128]{2,1,0:T(8,128)S(1)} fusion(f32[16,128]{1,0:T(8,128)} %bitcast.142, f32[16,128]{1,0:T(8,128)S(1)} %reduce_window_sum.51, f32[128,128]{1,0:T(8,128)S(1)} %bitcast.151, f32[128,128]{1,0:T(8,128)S(1)} %bitcast.148, pred[128,128]{1,0:T(8,128)(4,1)S(1)} %iota_compare_fusion.4), kind=kOutput, calls=%fused_computation.6.clone.1 | convolution fusion | flops 403701760 | bytes 1212416 | tf_op jit(solution)/shard_map/while/body/eval_jaxpr/hnt,hns->hts/dot_general | solution.py:59
  108.8 3.0 %fusion.106 = f32[3,16,64,128]{3,2,1,0:T(8,128)} fusion(f32[3,16,64,128]{3,2,1,0:T(8,128)} %get-tuple-element.298, s32[]{:T(128)} %get-tuple-element.296, f32[16,64,128]{2,1,0:T(8,128)S(1)} %fusion.104, f32[16,64,128]{2,1,0:T(8,128)S(1)} %bitcast.144, f32[16,128,128]{2,1,0:T(8,128)S(1)} %fusion.105), kind=kOutput, calls=%fused_computation.11.clone.1 | convolution fusion | flops 201457664 | bytes 2621952 | tf_op jit(solution)/shard_map/while/body/eval_jaxpr/hts,hps->hpt/dot_general | solution.py:63
  111.8 2.1 convolution_add_fusion.3
  113.9 1.4 constant_dynamic-slice_fusion.14
  117.2 1.6 fusion.104
  119.0 2.7 %fusion.105 = f32[16,128,128]{2,1,0:T(8,128)S(1)} fusion(f32[16,128]{1,0:T(8,128)} %bitcast.142, f32[16,128]{1,0:T(8,128)S(1)} %reduce_window_sum.51, f32[128,128]{1,0:T(8,128)S(1)} %bitcast.151, f32[128,128]{1,0:T(8,128)S(1)} %bitcast.148, pred[128,128]{1,0:T(8,128)(4,1)S(1)} %iota_compare_fusion.4), kind=kOutput, calls=%fused_computation.6.clone.1 | convolution fusion | flops 403701760 | bytes 1212416 | tf_op jit(solution)/shard_map/while/body/eval_jaxpr/hnt,hns->hts/dot_general | solution.py:59
  122.3 2.9 %fusion.106 = f32[3,16,64,128]{3,2,1,0:T(8,128)} fusion(f32[3,16,64,128]{3,2,1,0:T(8,128)} %get-tuple-element.298, s32[]{:T(128)} %get-tuple-element.296, f32[16,64,128]{2,1,0:T(8,128)S(1)} %fusion.104, f32[16,64,128]{2,1,0:T(8,128)S(1)} %bitcast.144, f32[16,128,128]{2,1,0:T(8,128)S(1)} %fusion.105), kind=kOutput, calls=%fused_computation.11.clone.1 | convolution fusion | flops 201457664 | bytes 2621952 | tf_op jit(solution)/shard_map/while/body/eval_jaxpr/hts,hps->hpt/dot_general | solution.py:63
  125.3 2.1 convolution_add_fusion.3
  128.2 1.3 dynamic-slice
  131.0 13.7 %all-reduce.1 = bf16[128]{0:T(256)(128)(2,1)S(1)} all-reduce(bf16[128]{0:T(256)(128)(2,1)S(1)} %dynamic-update-slice), channel_id=2, replica_groups=mesh['ep'=8,'tp'=4] {'ep'}, use_global_device_ids=true, to_apply=%add.1 | all-reduce | flops 128 | bytes 512
  149.7 7.9 %all-to-all-start.1 = ((bf16[512,8,80]{0,2,1:T(8,128)(2,1)}), bf16[512,8,80]{0,2,1:T(8,128)(2,1)S(1)}, u32[]{:S(2)}, u32[]{:S(2)}) async-start(bf16[512,8,80]{0,2,1:T(8,128)(2,1)} %bitcast.160), calls=%async_computation.2 | async-start | bytes 1310720 | tf_op jit(solution)/shard_map/all_to_all | solution.py:186
  157.6 30.3 %all-gather.7.cloned.1.call-done = bf16[128,64,128]{2,1,0:T(8,128)(2,1)} async-done(((bf16[16,64,128]{2,1,0:T(8,128)(2,1)}), bf16[128,64,128]{2,1,0:T(8,128)(2,1)}) %all-gather.7.cloned.1.call-update) | async-done | bytes 2097168 | tf_op jit(solution)/shard_map/all_gather | solution.py:26
  187.9 8.2 %while.25 = (s32[]{:T(128)}, f32[16,64,128]{2,1,0:T(8,128)S(1)}, s32[]{:T(128)}, bf16[8,16]{1,0:T(8,128)(2,1)S(1)}, bf16[8,16,64,128]{3,2,1,0:T(8,128)(2,1)}, /*index=5*/s32[]{:T(128)}, s32[]{:T(128)}, s32[]{:T(128)}) while((s32[]{:T(128)}, f32[16,64,128]{2,1,0:T(8,128)S(1)}, s32[]{:T(128)}, bf16[8,16]{1,0:T(8,128)(2,1)S(1)}, ...), condition=%wide.region_5.6_spmd, body=%wide.region_4.5_spmd.sunk | while | flops 393237 | bytes 1311007 | solution.py:40
  196.2 3.0 %multiply_reduce_fusion = (f32[16,384]{1,0:T(8,128)S(1)}, f32[16,64,384]{2,1,0:T(8,128)S(1)}) fusion(bf16[16,64,384]{2,1,0:T(8,128)(2,1)} %bitcast.168, f32[16,384]{1,0:T(8,128)S(1)} %copy_bitcast_fusion, f32[16,64,128]{2,1,0:T(8,128)S(1)} %get-tuple-element.91, f32[128,384]{0,1:T(8,128)S(1)} %bitcast.155, f32[3,16,64,128]{3,2,1,0:T(8,128)S(1)} %copy-done.20), kind=kOutput, calls=%fused_computation.62 | convolution fusion | flops 607905792 | bytes 4702208 | tf_op jit(solution)/shard_map/nt,hpn->hpt/dot_general | solution.py:132
  200.4 2.0 gather_fusion
  202.8 1.5 multiply_reduce_fusion.2
  (180 shorter events, 32.2 us)
Async XLA Ops:
  8.0 54.8 %all-gather.5.cloned.1.call-start = ((), (), s32[]{:S(2)}) async-start(), calls=%async_computation.3 | async-start | bytes 3276800 | tf_op jit(solution)/shard_map/all_gather | solution.py:170
  11.4 25.2 %copy-start.13 = (s32[320]{0:T(512)}, s32[320]{0:T(512)S(1)}, u32[]{:S(2)}) copy-start(s32[320]{0:T(512)S(1)} %get-tuple-element.186) | copy-start | bytes 3844
  12.2 24.5 %copy-start.9 = (bf16[256,384]{1,0:T(8,128)(2,1)S(1)}, bf16[256,384]{1,0:T(8,128)(2,1)}, u32[]{:S(2)}) copy-start(bf16[256,384]{1,0:T(8,128)(2,1)} %param.26) | copy-start | bytes 589828
  12.2 24.5 %copy-start.10 = (bf16[256,384]{1,0:T(8,128)(2,1)S(1)}, bf16[256,384]{1,0:T(8,128)(2,1)}, u32[]{:S(2)}) copy-start(bf16[256,384]{1,0:T(8,128)(2,1)} %param.25) | copy-start | bytes 589828
  12.3 24.7 %copy-start.1 = (bf16[1024,384]{1,0:T(8,128)(2,1)S(1)}, bf16[1024,384]{1,0:T(8,128)(2,1)}, u32[]{:S(2)}) copy-start(bf16[1024,384]{1,0:T(8,128)(2,1)} %param.21) | copy-start | bytes 2359300
  15.7 23.1 %copy-start.17 = (f32[256,4]{0,1:T(4,128)S(1)}, f32[256,4]{0,1:T(4,128)}, u32[]{:S(2)}) copy-start(f32[256,4]{0,1:T(4,128)} %param.29) | copy-start | bytes 12292
  15.7 23.1 %copy-start.18 = (f32[256,4]{0,1:T(4,128)S(1)}, f32[256,4]{0,1:T(4,128)}, u32[]{:S(2)}) copy-start(f32[256,4]{0,1:T(4,128)} %param.28) | copy-start | bytes 12292
  15.7 23.1 %copy-start.12 = (f32[1024,4]{0,1:T(4,128)S(1)}, f32[1024,4]{0,1:T(4,128)}, u32[]{:S(2)}) copy-start(f32[1024,4]{0,1:T(4,128)} %param.27) | copy-start | bytes 49156
  15.7 23.1 %copy-start.11 = (f32[16,384]{1,0:T(8,128)S(1)}, f32[16,384]{1,0:T(8,128)}, u32[]{:S(2)}) copy-start(f32[16,384]{1,0:T(8,128)} %param.23) | copy-start | bytes 73732
  15.7 23.1 %copy-start.19 = (f32[16]{0:T(128)S(1)}, f32[16]{0:T(128)}, u32[]{:S(2)}) copy-start(f32[16]{0:T(128)} %param.24) | copy-start | bytes 196
  36.6 113.1 %reduce-scatter.2.cloned.1.call-start = ((), (), s32[]{:S(2)}) async-start(), calls=%async_computation.4 | async-start | bytes 3276800 | tf_op jit(solution)/shard_map/reduce_scatter | solution.py:177
  37.3 4.4 %collective-permute-start = (bf16[1280,3]{0,1:T(4,128)(2,1)S(1)}, bf16[1280,3]{0,1:T(4,128)(2,1)S(1)}, u32[]{:S(2)}, u32[]{:S(2)}) collective-permute-start(bf16[1280,3]{0,1:T(4,128)(2,1)S(1)} %pad_maximum_fusion.3), channel_id=1, source_target_pairs={{0,4},{4,8},{8,12},{12,16},{16,20},{20,24},{24,28},{1,5},{5,9},{9,... | collective-permute-start | bytes 23048 | tf_op jit(solution)/shard_map/ppermute | solution.py:20
  39.6 2.3 %copy-start.4 = (f32[16,384]{1,0:T(8,128)}, f32[16,384]{1,0:T(8,128)S(1)}, u32[]{:S(2)}) copy-start(f32[16,384]{1,0:T(8,128)S(1)} %get-tuple-element.162) | copy-start | bytes 73732
  45.2 2.8 %copy-start.15 = (f32[128]{0:T(128)S(1)}, f32[128]{0:T(128)}, u32[]{:S(2)}) copy-start(f32[128]{0:T(128)} %get-tuple-element.178) | copy-start | bytes 1540
  45.2 2.8 %copy-start.16 = (f32[128]{0:T(128)S(1)}, f32[128]{0:T(128)}, u32[]{:S(2)}) copy-start(f32[128]{0:T(128)} %get-tuple-element.179) | copy-start | bytes 1540
  86.5 101.4 %all-gather.7.cloned.1.call-start = ((), (), s32[]{:S(2)}) async-start(), calls=%async_computation.5 | async-start | bytes 2359296 | tf_op jit(solution)/shard_map/all_gather | solution.py:26
  86.8 3.2 %copy-start.5 = (f32[3,16,128]{2,0,1:T(4,128)}, f32[3,16,128]{2,0,1:T(4,128)S(1)}, u32[]{:S(2)}) copy-start(f32[3,16,128]{2,0,1:T(4,128)S(1)} %get-tuple-element.310) | copy-start | bytes 73732 | tf_op jit(solution)/shard_map/while
  86.8 3.3 %copy-start.2 = (f32[3,128,128]{1,2,0:T(8,128)}, f32[3,128,128]{1,2,0:T(8,128)S(1)}, u32[]{:S(2)}) copy-start(f32[3,128,128]{1,2,0:T(8,128)S(1)} %get-tuple-element.313) | copy-start | bytes 589828 | tf_op jit(solution)/shard_map/while
  95.2 3.0 %copy-start.8 = (f32[16]{0:T(128)S(1)}, f32[16]{0:T(128)}, u32[]{:S(2)}) copy-start(f32[16]{0:T(128)} %copy-done.7) | copy-start | bytes 196 | tf_op jit(solution)/shard_map/while
  95.2 5.1 %copy-start.6 = (f32[3,16,128]{2,0,1:T(4,128)S(1)}, f32[3,16,128]{2,0,1:T(4,128)}, u32[]{:S(2)}) copy-start(f32[3,16,128]{2,0,1:T(4,128)} %copy-done.5) | copy-start | bytes 73732 | tf_op jit(solution)/shard_map/while
  98.2 2.2 %copy-start.3 = (f32[3,128,128]{1,2,0:T(8,128)S(1)}, f32[3,128,128]{1,2,0:T(8,128)}, u32[]{:S(2)}) copy-start(f32[3,128,128]{1,2,0:T(8,128)} %copy-done.2) | copy-start | bytes 589828 | tf_op jit(solution)/shard_map/while
  100.4 3.2 %copy-start.5 = (f32[3,16,128]{2,0,1:T(4,128)}, f32[3,16,128]{2,0,1:T(4,128)S(1)}, u32[]{:S(2)}) copy-start(f32[3,16,128]{2,0,1:T(4,128)S(1)} %get-tuple-element.310) | copy-start | bytes 73732 | tf_op jit(solution)/shard_map/while
  100.4 3.3 %copy-start.2 = (f32[3,128,128]{1,2,0:T(8,128)}, f32[3,128,128]{1,2,0:T(8,128)S(1)}, u32[]{:S(2)}) copy-start(f32[3,128,128]{1,2,0:T(8,128)S(1)} %get-tuple-element.313) | copy-start | bytes 589828 | tf_op jit(solution)/shard_map/while
  108.7 3.0 %copy-start.8 = (f32[16]{0:T(128)S(1)}, f32[16]{0:T(128)}, u32[]{:S(2)}) copy-start(f32[16]{0:T(128)} %copy-done.7) | copy-start | bytes 196 | tf_op jit(solution)/shard_map/while
  108.7 5.1 %copy-start.6 = (f32[3,16,128]{2,0,1:T(4,128)S(1)}, f32[3,16,128]{2,0,1:T(4,128)}, u32[]{:S(2)}) copy-start(f32[3,16,128]{2,0,1:T(4,128)} %copy-done.5) | copy-start | bytes 73732 | tf_op jit(solution)/shard_map/while
  111.7 2.2 %copy-start.3 = (f32[3,128,128]{1,2,0:T(8,128)S(1)}, f32[3,128,128]{1,2,0:T(8,128)}, u32[]{:S(2)}) copy-start(f32[3,128,128]{1,2,0:T(8,128)} %copy-done.2) | copy-start | bytes 589828 | tf_op jit(solution)/shard_map/while
  113.9 3.2 %copy-start.5 = (f32[3,16,128]{2,0,1:T(4,128)}, f32[3,16,128]{2,0,1:T(4,128)S(1)}, u32[]{:S(2)}) copy-start(f32[3,16,128]{2,0,1:T(4,128)S(1)} %get-tuple-element.310) | copy-start | bytes 73732 | tf_op jit(solution)/shard_map/while
  113.9 3.3 %copy-start.2 = (f32[3,128,128]{1,2,0:T(8,128)}, f32[3,128,128]{1,2,0:T(8,128)S(1)}, u32[]{:S(2)}) copy-start(f32[3,128,128]{1,2,0:T(8,128)S(1)} %get-tuple-element.313) | copy-start | bytes 589828 | tf_op jit(solution)/shard_map/while
  122.3 3.0 %copy-start.8 = (f32[16]{0:T(128)S(1)}, f32[16]{0:T(128)}, u32[]{:S(2)}) copy-start(f32[16]{0:T(128)} %copy-done.7) | copy-start | bytes 196 | tf_op jit(solution)/shard_map/while
  122.3 5.1 %copy-start.6 = (f32[3,16,128]{2,0,1:T(4,128)S(1)}, f32[3,16,128]{2,0,1:T(4,128)}, u32[]{:S(2)}) copy-start(f32[3,16,128]{2,0,1:T(4,128)} %copy-done.5) | copy-start | bytes 73732 | tf_op jit(solution)/shard_map/while
  149.7 50.7 %all-to-all-start.1 = ((bf16[512,8,80]{0,2,1:T(8,128)(2,1)}), bf16[512,8,80]{0,2,1:T(8,128)(2,1)S(1)}, u32[]{:S(2)}, u32[]{:S(2)}) async-start(bf16[512,8,80]{0,2,1:T(8,128)(2,1)} %bitcast.160), calls=%async_computation.2 | async-start | bytes 1310720 | tf_op jit(solution)/shard_map/all_to_all | solution.py:186
  187.9 8.3 %copy-start.20 = (f32[3,16,64,128]{3,2,1,0:T(8,128)S(1)}, f32[3,16,64,128]{3,2,1,0:T(8,128)}, u32[]{:S(2)}) copy-start(f32[3,16,64,128]{3,2,1,0:T(8,128)} %get-tuple-element.89) | copy-start | bytes 4718596
  (6 other events, 9.0 us)
Sparse Core Ops, SparseCore 0:
  36.7 26.0 all-gather.4
  86.6 33.8 reduce-scatter.1
Sparse Core Ops, SparseCore 1:
  128.3 59.6 all-gather.6
where the time goes:
time: 213 us; the launch traced here: 212 us
  matrix products  55.1 us (26%)
  waiting for transfers between devices  45.8 us (22%)
  blocking collectives  34.5 us (16%)
  other arithmetic  26.1 us (12%)
  local copies, waits for them, and re-layouts  23.2 us (11%)
  between operations  16.7 us (8%)
  starting transfers between devices  9.75 us (5%)
    all_gather x1, waiting for transfers between devices, carried_in(): lax.all_gather(a.astype(kind), axis)  30.3 us
    all_to_all x1, blocking collectives, experts_half(): lax.all_to_all(outbox.reshape(experts, capacity, col_width), 'ep', split_...  20.8 us
    dot_general x1, matrix products, experts_half(): lax.dot_general(columns, hidden, (((0,), (1,)), ((), ())), preferred_elem...  15.2 us
    all_gather x1, waiting for transfers between devices, experts_half(): part_rows = lax.all_gather(arrived, 'tp', axis=1, tiled=True)  14.7 us
    unnamed x1, blocking collectives  13.7 us
    dot_general x3, matrix products, block_step(): inner_term = jnp.einsum('hts,hps->hpt', scores, x_block, precision=HIGHEST)  8.92 us
    dot_general x1, matrix products, experts_half(): gate_act = jnp.dot(part_rows, gate_rows, preferred_element_type=jnp.float32)  8.51 us
    dot_general x3, matrix products, block_step(): jnp.einsum('hnt,hns->hts', c_block, b_block, precision=HIGHEST) * decay_mask  8.14 us
  transfers between devices with their start and end apart: 5, of which 3 were waited for; matrix products, arithmetic and copies ran while one was open for 33% of the time, Pallas kernels for 0%

commit v1 on v0

--- a/solution.py
+++ b/solution.py
@@ -167,7 +167,8 @@
     arrived = lax.all_to_all(
         outbox.reshape(experts, capacity, col_width), "ep", split_axis=0, concat_axis=0, tiled=True
     ).reshape(-1, col_width)
-    part_rows = lax.all_gather(arrived, "tp", axis=1, tiled=True)
+    shards = lax.all_gather(arrived, "tp", axis=0, tiled=False)
+    part_rows = jnp.concatenate(shards, axis=1)
     gate_rows = w_gate[0]
     up_rows = w_up[0]
     gate_act = jnp.dot(part_rows, gate_rows, preferred_element_type=jnp.float32)

time: 213 us -> 209 us (0.981)
  matrix products: 55.1 us -> 49.8 us
  local copies, waits for them, and re-layouts: 23.2 us -> 26.6 us
    dot_general x1, matrix products: 15.2 us -> 4.82 us  [experts_half(): lax.dot_general(columns, hidden, (((0,), (1,)), ((), ())), preferred_elem...]
    dot_general x0 -> x1, matrix products: none -> 6.54 us  [experts_half(): up_act = jnp.dot(part_rows, up_rows, preferred_element_type=jnp.float32)]
    all_gather x0 -> x1, local copies, waits for them, and re-layouts: none -> 4.4 us  [experts_half(): shards = lax.all_gather(arrived, 'tp', axis=0, tiled=False)]
  transfers between devices with their start and end apart: 5 -> 5, of which waited for: 3 -> 3; matrix products, arithmetic and copies ran while one was open for 33% -> 32% of each run, Pallas kernels for 0% -> 0%
where the time goes in v1:
time: 209 us; the launch traced here: 207 us
  matrix products  49.8 us (24%)
  waiting for transfers between devices  45.1 us (22%)
  blocking collectives  34.4 us (16%)
  local copies, waits for them, and re-layouts  26.6 us (13%)
  other arithmetic  24.2 us (12%)
  between operations  16.8 us (8%)
  starting transfers between devices  9.75 us (5%)
    all_gather x1, waiting for transfers between devices, carried_in(): lax.all_gather(a.astype(kind), axis)  30.2 us
    all_to_all x1, blocking collectives, experts_half(): lax.all_to_all(outbox.reshape(experts, capacity, col_width), 'ep', split_...  20.8 us
    all_gather x1, waiting for transfers between devices, experts_half(): shards = lax.all_gather(arrived, 'tp', axis=0, tiled=False)  14.7 us
    unnamed x1, blocking collectives  13.6 us
    dot_general x3, matrix products, block_step(): inner_term = jnp.einsum('hts,hps->hpt', scores, x_block, precision=HIGHEST)  8.88 us
    dot_general x3, matrix products, block_step(): jnp.einsum('hnt,hns->hts', c_block, b_block, precision=HIGHEST) * decay_mask  8.14 us
    all_to_all x1, starting transfers between devices, experts_half(): lax.all_to_all(expert_out, 'ep', split_axis=1, concat_axis=1, tiled=True)  7.93 us
    add x7, other arithmetic, combine_states(): after_part[0][..., None, None] * before_part[1] + after_part[1]  7.88 us
  transfers between devices with their start and end apart: 5, of which 3 were waited for; matrix products, arithmetic and copies ran while one was open for 32% of the time, Pallas kernels for 0%

profile of v1, /device:TPU:31, one launch (start us, length us, event | category | flops | bytes accessed | tf_op | source)
XLA Modules:
  0.0 207.2 jit_solution(14683823329358027904)
XLA Ops:
  8.1 1.3 convert_element_type.100
  12.3 3.4 %scatter_custom_fusion = bf16[640,512]{1,0:T(8,128)(2,1)S(1)} fusion(s32[320]{0:T(512)S(1)} %get-tuple-element.194, bf16[160,512]{1,0:T(8,128)(2,1)S(1)} %fusion.45, s32[1024]{0:T(1024)S(1)} %pad_clamp_fusion.1, bf16[]{:T(256)} %constant.124.clone.1), kind=kCustom, calls=%fused_computation.70 | custom fusion | bytes 655362 | tf_op jit(solution)/shard_map/scatter | solution.py:165
  15.8 20.8 %all_to_all.10 = bf16[8,80,512]{2,1,0:T(8,128)(2,1)} all-to-all(bf16[8,80,512]{2,1,0:T(8,128)(2,1)S(1)} %bitcast.157), channel_id=1, replica_groups=mesh['ep'=8,'tp'=4] {'ep'}, dimensions={0} | all-to-all | bytes 1310720 | tf_op jit(solution)/shard_map/all_to_all | solution.py:167
  37.3 1.5 collective-permute-start
  42.0 3.2 %divide_multiply_fusion = f32[1024,384]{1,0:T(8,128)} fusion(f32[1024,384]{1,0:T(8,128)S(1)} %convert_element_type.89, f32[1024,3]{1,0:T(8,128)S(1)} %copy.59, f32[1024]{0:T(1024)S(1)} %bitcast.169, f32[1024]{0:T(1024)S(1)} %bitcast.170, f32[1024]{0:T(1024)S(1)} %bitcast.168, f32[1024]{0:T(1024)S(1)} %bitcast.167), kind=kLoop, calls=%fused_computation.63 | loop fusion | flops 5505024 | bytes 3174400 | tf_op jit(solution)/shard_map/jit(silu)/mul | solution.py:50
  45.2 2.6 %reshape_reshape.3 = f32[16,64,3,128]{3,2,1,0:T(4,128)S(1)} reshape(f32[1024,384]{1,0:T(8,128)} %divide_multiply_fusion) | data formatting | bytes 3145728 | tf_op jit(solution)/shard_map/reshape;reshape | solution.py:105
  48.1 14.7 %all-gather.5.cloned.1.call-done = bf16[4,640,512]{2,1,0:T(8,128)(2,1)} async-done(((bf16[1,640,512]{2,1,0:T(8,128)(2,1)}), bf16[4,640,512]{2,1,0:T(8,128)(2,1)}) %all-gather.5.cloned.1.call-update) | async-done | bytes 2621456 | tf_op jit(solution)/shard_map/all_gather | solution.py:170
  62.8 4.4 %copy.71 = bf16[4,640,512]{1,2,0:T(8,128)(2,1)} copy(bf16[4,640,512]{2,1,0:T(8,128)(2,1)} %all-gather.5.cloned.1.call-done) | data formatting | bytes 5242880 | tf_op jit(solution)/shard_map/all_gather | solution.py:170
  67.2 7.0 %fusion.18 = f32[640,1280]{1,0:T(8,128)S(1)} fusion(bf16[640,2048]{0,1:T(8,128)(2,1)} %bitcast.154, bf16[1,2048,1280]{2,1,0:T(8,128)(2,1)} %param.35), kind=kOutput, calls=%fused_computation.35 | convolution fusion | flops 3355443200 | bytes 11141120 | tf_op jit(solution)/shard_map/dot_general | solution.py:174
  74.3 6.5 %fusion.26 = bf16[640,1280]{1,0:T(8,128)(2,1)S(1)} fusion(bf16[640,2048]{0,1:T(8,128)(2,1)S(1)} %bitcast.155, bf16[1,2048,1280]{2,1,0:T(8,128)(2,1)} %param.36, f32[640,1280]{1,0:T(8,128)S(1)} %fusion.18), kind=kOutput, calls=%fused_computation.39 | convolution fusion | flops 3360358400 | bytes 12779520 | tf_op jit(solution)/shard_map/dot_general | solution.py:175
  80.9 4.8 %fusion.29 = bf16[2048,640]{0,1:T(8,128)(2,1)} fusion(bf16[640,1280]{1,0:T(8,128)(2,1)S(1)} %fusion.26, bf16[1,1280,2048]{2,1,0:T(8,128)(2,1)S(1)} %bitcast.174), kind=kOutput, calls=%fused_computation.40 | convolution fusion | flops 3356753920 | bytes 9502720 | tf_op jit(solution)/shard_map/dot_general | solution.py:179
  86.0 36.9 %while.26 = (s32[]{:T(128)}, f32[16,64,128]{2,1,0:T(8,128)S(1)}, f32[3,16,64,128]{3,2,1,0:T(8,128)}, f32[3,16,128]{2,0,1:T(4,128)}, f32[3,16,64,128]{3,0,2,1:T(4...) while((s32[]{:T(128)}, f32[16,64,128]{2,1,0:T(8,128)S(1)}, ...), condition=%wide.region_2.3_spmd.clone, body=%wide.region_0.2_spmd.clone.sunk | while | flops 1008879616 | bytes 9881236 | solution.py:117
  88.1 1.6 fusion.102
  89.9 2.7 %fusion.103 = f32[16,128,128]{2,1,0:T(8,128)S(1)} fusion(f32[16,128]{1,0:T(8,128)} %bitcast.164, f32[16,128]{1,0:T(8,128)S(1)} %reduce_window_sum.51, f32[128,128]{1,0:T(8,128)S(1)} %bitcast.153, f32[128,128]{1,0:T(8,128)S(1)} %bitcast.150, pred[128,128]{1,0:T(8,128)(4,1)S(1)} %iota_compare_fusion.4), kind=kOutput, calls=%fused_computation.6.clone.1 | convolution fusion | flops 403701760 | bytes 1212416 | tf_op jit(solution)/shard_map/while/body/eval_jaxpr/hnt,hns->hts/dot_general | solution.py:59
  93.2 3.0 %fusion.104 = f32[3,16,64,128]{3,2,1,0:T(8,128)} fusion(f32[3,16,64,128]{3,2,1,0:T(8,128)} %get-tuple-element.306, s32[]{:T(128)} %get-tuple-element.304, f32[16,64,128]{2,1,0:T(8,128)S(1)} %fusion.102, f32[16,64,128]{2,1,0:T(8,128)S(1)} %bitcast.146, f32[16,128,128]{2,1,0:T(8,128)S(1)} %fusion.103), kind=kOutput, calls=%fused_computation.11.clone.1 | convolution fusion | flops 201457664 | bytes 2621952 | tf_op jit(solution)/shard_map/while/body/eval_jaxpr/hts,hps->hpt/dot_general | solution.py:63
  96.1 2.1 %convolution_add_fusion.3 = f32[16,64,128]{2,1,0:T(8,128)S(1)} fusion(f32[128,128]{1,0:T(8,128)S(1)} %bitcast.151, f32[16,64,128]{2,1,0:T(8,128)S(1)} %bitcast.147, f32[16,64,128]{2,1,0:T(8,128)S(1)} %get-tuple-element.305, f32[16,128]{1,0:T(8,128)S(1)} %get-tuple-element.290, f32[16]{0:T(128)S(1)} %exp.116, pred[]{:T(512)S(6)} %compare.10), kind=kOutput, calls=%fused_computation.12.clone.1 | convolution fusion | flops 201850880 | bytes 1646657 | tf_op jit(solution)/shard_map/while/body/eval_jaxpr/hps,hns->hpn/dot_general | solution.py:69
  100.4 1.6 fusion.102
  102.2 2.7 %fusion.103 = f32[16,128,128]{2,1,0:T(8,128)S(1)} fusion(f32[16,128]{1,0:T(8,128)} %bitcast.164, f32[16,128]{1,0:T(8,128)S(1)} %reduce_window_sum.51, f32[128,128]{1,0:T(8,128)S(1)} %bitcast.153, f32[128,128]{1,0:T(8,128)S(1)} %bitcast.150, pred[128,128]{1,0:T(8,128)(4,1)S(1)} %iota_compare_fusion.4), kind=kOutput, calls=%fused_computation.6.clone.1 | convolution fusion | flops 403701760 | bytes 1212416 | tf_op jit(solution)/shard_map/while/body/eval_jaxpr/hnt,hns->hts/dot_general | solution.py:59
  105.5 3.0 %fusion.104 = f32[3,16,64,128]{3,2,1,0:T(8,128)} fusion(f32[3,16,64,128]{3,2,1,0:T(8,128)} %get-tuple-element.306, s32[]{:T(128)} %get-tuple-element.304, f32[16,64,128]{2,1,0:T(8,128)S(1)} %fusion.102, f32[16,64,128]{2,1,0:T(8,128)S(1)} %bitcast.146, f32[16,128,128]{2,1,0:T(8,128)S(1)} %fusion.103), kind=kOutput, calls=%fused_computation.11.clone.1 | convolution fusion | flops 201457664 | bytes 2621952 | tf_op jit(solution)/shard_map/while/body/eval_jaxpr/hts,hps->hpt/dot_general | solution.py:63
  108.4 2.1 %convolution_add_fusion.3 = f32[16,64,128]{2,1,0:T(8,128)S(1)} fusion(f32[128,128]{1,0:T(8,128)S(1)} %bitcast.151, f32[16,64,128]{2,1,0:T(8,128)S(1)} %bitcast.147, f32[16,64,128]{2,1,0:T(8,128)S(1)} %get-tuple-element.305, f32[16,128]{1,0:T(8,128)S(1)} %get-tuple-element.290, f32[16]{0:T(128)S(1)} %exp.116, pred[]{:T(512)S(6)} %compare.10), kind=kOutput, calls=%fused_computation.12.clone.1 | convolution fusion | flops 201850880 | bytes 1646657 | tf_op jit(solution)/shard_map/while/body/eval_jaxpr/hps,hns->hpn/dot_general | solution.py:69
  112.7 1.6 fusion.102
  114.5 2.7 %fusion.103 = f32[16,128,128]{2,1,0:T(8,128)S(1)} fusion(f32[16,128]{1,0:T(8,128)} %bitcast.164, f32[16,128]{1,0:T(8,128)S(1)} %reduce_window_sum.51, f32[128,128]{1,0:T(8,128)S(1)} %bitcast.153, f32[128,128]{1,0:T(8,128)S(1)} %bitcast.150, pred[128,128]{1,0:T(8,128)(4,1)S(1)} %iota_compare_fusion.4), kind=kOutput, calls=%fused_computation.6.clone.1 | convolution fusion | flops 403701760 | bytes 1212416 | tf_op jit(solution)/shard_map/while/body/eval_jaxpr/hnt,hns->hts/dot_general | solution.py:59
  117.7 3.0 %fusion.104 = f32[3,16,64,128]{3,2,1,0:T(8,128)} fusion(f32[3,16,64,128]{3,2,1,0:T(8,128)} %get-tuple-element.306, s32[]{:T(128)} %get-tuple-element.304, f32[16,64,128]{2,1,0:T(8,128)S(1)} %fusion.102, f32[16,64,128]{2,1,0:T(8,128)S(1)} %bitcast.146, f32[16,128,128]{2,1,0:T(8,128)S(1)} %fusion.103), kind=kOutput, calls=%fused_computation.11.clone.1 | convolution fusion | flops 201457664 | bytes 2621952 | tf_op jit(solution)/shard_map/while/body/eval_jaxpr/hts,hps->hpt/dot_general | solution.py:63
  120.7 2.1 %convolution_add_fusion.3 = f32[16,64,128]{2,1,0:T(8,128)S(1)} fusion(f32[128,128]{1,0:T(8,128)S(1)} %bitcast.151, f32[16,64,128]{2,1,0:T(8,128)S(1)} %bitcast.147, f32[16,64,128]{2,1,0:T(8,128)S(1)} %get-tuple-element.305, f32[16,128]{1,0:T(8,128)S(1)} %get-tuple-element.290, f32[16]{0:T(128)S(1)} %exp.116, pred[]{:T(512)S(6)} %compare.10), kind=kOutput, calls=%fused_computation.12.clone.1 | convolution fusion | flops 201850880 | bytes 1646657 | tf_op jit(solution)/shard_map/while/body/eval_jaxpr/hps,hns->hpn/dot_general | solution.py:69
  123.6 1.3 dynamic-slice
  126.5 13.6 %all-reduce.1 = bf16[128]{0:T(256)(128)(2,1)S(1)} all-reduce(bf16[128]{0:T(256)(128)(2,1)S(1)} %dynamic-update-slice), channel_id=2, replica_groups=mesh['ep'=8,'tp'=4] {'ep'}, use_global_device_ids=true, to_apply=%add.1 | all-reduce | flops 128 | bytes 512
  145.1 7.9 %all-to-all-start.1 = ((bf16[512,8,80]{0,2,1:T(8,128)(2,1)}), bf16[512,8,80]{0,2,1:T(8,128)(2,1)S(1)}, u32[]{:S(2)}, u32[]{:S(2)}) async-start(bf16[512,8,80]{0,2,1:T(8,128)(2,1)} %bitcast.166), calls=%async_computation.2 | async-start | bytes 1310720 | tf_op jit(solution)/shard_map/all_to_all | solution.py:187
  153.1 30.2 %all-gather.7.cloned.1.call-done = bf16[128,64,128]{2,1,0:T(8,128)(2,1)} async-done(((bf16[16,64,128]{2,1,0:T(8,128)(2,1)}), bf16[128,64,128]{2,1,0:T(8,128)(2,1)}) %all-gather.7.cloned.1.call-update) | async-done | bytes 2097168 | tf_op jit(solution)/shard_map/all_gather | solution.py:26
  183.3 8.2 %while.25 = (s32[]{:T(128)}, f32[16,64,128]{2,1,0:T(8,128)S(1)}, s32[]{:T(128)}, bf16[8,16]{1,0:T(8,128)(2,1)S(1)}, bf16[8,16,64,128]{3,2,1,0:T(8,128)(2,1)}, /*index=5*/s32[]{:T(128)}, s32[]{:T(128)}, s32[]{:T(128)}) while((s32[]{:T(128)}, f32[16,64,128]{2,1,0:T(8,128)S(1)}, s32[]{:T(128)}, bf16[8,16]{1,0:T(8,128)(2,1)S(1)}, ...), condition=%wide.region_5.6_spmd, body=%wide.region_4.5_spmd.sunk | while | flops 393237 | bytes 1311007 | solution.py:40
  191.6 3.0 %multiply_reduce_fusion = (f32[16,384]{1,0:T(8,128)S(1)}, f32[16,64,384]{2,1,0:T(8,128)S(1)}) fusion(bf16[16,64,384]{2,1,0:T(8,128)(2,1)} %bitcast.175, f32[16,384]{1,0:T(8,128)S(1)} %copy_bitcast_fusion, f32[16,64,128]{2,1,0:T(8,128)S(1)} %get-tuple-element.91, f32[128,384]{0,1:T(8,128)S(1)} %bitcast.159, f32[3,16,64,128]{3,2,1,0:T(8,128)S(1)} %copy-done.20), kind=kOutput, calls=%fused_computation.62 | convolution fusion | flops 607905792 | bytes 4702208 | tf_op jit(solution)/shard_map/nt,hpn->hpt/dot_general | solution.py:132
  195.8 2.0 gather_fusion
  198.3 1.5 multiply_reduce_fusion.2
  (183 shorter events, 31.5 us)
Async XLA Ops:
  8.0 1.3 copy-start.1
  8.0 1.6 copy-start.14
  8.0 54.8 %all-gather.5.cloned.1.call-start = ((), (), s32[]{:S(2)}) async-start(), calls=%async_computation.3 | async-start | bytes 3276800 | tf_op jit(solution)/shard_map/all_gather | solution.py:170
  11.4 25.2 %copy-start.13 = (s32[320]{0:T(512)}, s32[320]{0:T(512)S(1)}, u32[]{:S(2)}) copy-start(s32[320]{0:T(512)S(1)} %get-tuple-element.194) | copy-start | bytes 3844
  12.2 24.5 %copy-start.9 = (bf16[256,384]{1,0:T(8,128)(2,1)S(1)}, bf16[256,384]{1,0:T(8,128)(2,1)}, u32[]{:S(2)}) copy-start(bf16[256,384]{1,0:T(8,128)(2,1)} %param.26) | copy-start | bytes 589828
  12.2 24.5 %copy-start.10 = (bf16[256,384]{1,0:T(8,128)(2,1)S(1)}, bf16[256,384]{1,0:T(8,128)(2,1)}, u32[]{:S(2)}) copy-start(bf16[256,384]{1,0:T(8,128)(2,1)} %param.25) | copy-start | bytes 589828
  12.3 24.7 %copy-start.2 = (bf16[1024,384]{1,0:T(8,128)(2,1)S(1)}, bf16[1024,384]{1,0:T(8,128)(2,1)}, u32[]{:S(2)}) copy-start(bf16[1024,384]{1,0:T(8,128)(2,1)} %param.21) | copy-start | bytes 2359300
  15.7 23.1 %copy-start.17 = (f32[256,4]{0,1:T(4,128)S(1)}, f32[256,4]{0,1:T(4,128)}, u32[]{:S(2)}) copy-start(f32[256,4]{0,1:T(4,128)} %param.29) | copy-start | bytes 12292
  15.7 23.1 %copy-start.18 = (f32[256,4]{0,1:T(4,128)S(1)}, f32[256,4]{0,1:T(4,128)}, u32[]{:S(2)}) copy-start(f32[256,4]{0,1:T(4,128)} %param.28) | copy-start | bytes 12292
  15.7 23.1 %copy-start.12 = (f32[1024,4]{0,1:T(4,128)S(1)}, f32[1024,4]{0,1:T(4,128)}, u32[]{:S(2)}) copy-start(f32[1024,4]{0,1:T(4,128)} %param.27) | copy-start | bytes 49156
  15.7 23.1 %copy-start.11 = (f32[16,384]{1,0:T(8,128)S(1)}, f32[16,384]{1,0:T(8,128)}, u32[]{:S(2)}) copy-start(f32[16,384]{1,0:T(8,128)} %param.23) | copy-start | bytes 73732
  15.7 23.1 %copy-start.19 = (f32[16]{0:T(128)S(1)}, f32[16]{0:T(128)}, u32[]{:S(2)}) copy-start(f32[16]{0:T(128)} %param.24) | copy-start | bytes 196
  36.6 108.6 %reduce-scatter.2.cloned.1.call-start = ((), (), s32[]{:S(2)}) async-start(), calls=%async_computation.4 | async-start | bytes 3276800 | tf_op jit(solution)/shard_map/reduce_scatter | solution.py:178
  37.3 4.4 %collective-permute-start = (bf16[1280,3]{0,1:T(4,128)(2,1)S(1)}, bf16[1280,3]{0,1:T(4,128)(2,1)S(1)}, u32[]{:S(2)}, u32[]{:S(2)}) collective-permute-start(bf16[1280,3]{0,1:T(4,128)(2,1)S(1)} %pad_maximum_fusion.3), channel_id=1, source_target_pairs={{0,4},{4,8},{8,12},{12,16},{16,20},{20,24},{24,28},{1,5},{5,9},{9,... | collective-permute-start | bytes 23048 | tf_op jit(solution)/shard_map/ppermute | solution.py:20
  39.6 2.3 %copy-start.6 = (f32[16,384]{1,0:T(8,128)}, f32[16,384]{1,0:T(8,128)S(1)}, u32[]{:S(2)}) copy-start(f32[16,384]{1,0:T(8,128)S(1)} %get-tuple-element.170) | copy-start | bytes 73732
  45.2 2.8 %copy-start.15 = (f32[128]{0:T(128)S(1)}, f32[128]{0:T(128)}, u32[]{:S(2)}) copy-start(f32[128]{0:T(128)} %get-tuple-element.186) | copy-start | bytes 1540
  45.2 2.8 %copy-start.16 = (f32[128]{0:T(128)S(1)}, f32[128]{0:T(128)}, u32[]{:S(2)}) copy-start(f32[128]{0:T(128)} %get-tuple-element.187) | copy-start | bytes 1540
  67.2 7.1 %copy-start = (bf16[4,640,512]{1,2,0:T(8,128)(2,1)S(1)}, bf16[4,640,512]{1,2,0:T(8,128)(2,1)}, u32[]{:S(2)}) copy-start(bf16[4,640,512]{1,2,0:T(8,128)(2,1)} %copy.71) | copy-start | bytes 7864324
  67.2 13.6 %slice-start = ((s8[5242880]{0:T(1024)(128)(4,1)}), s8[4194304]{0:T(1024)(128)(4,1)S(1)}, s32[]{:S(2)}) async-start(s8[5242880]{0:T(1024)(128)(4,1)} %bitcast.173), calls=%async_computation.6 | async-start | bytes 8388608
  74.3 6.6 %slice-start.1 = ((s8[5242880]{0:T(1024)(128)(4,1)}), s8[1048576]{0:T(1024)(128)(4,1)S(1)}, s32[]{:S(2)}) async-start(s8[5242880]{0:T(1024)(128)(4,1)} %bitcast.173), calls=%async_computation.7 | async-start | bytes 2097152
  85.7 97.6 %all-gather.7.cloned.1.call-start = ((), (), s32[]{:S(2)}) async-start(), calls=%async_computation.5 | async-start | bytes 2359296 | tf_op jit(solution)/shard_map/all_gather | solution.py:26
  86.0 2.1 %copy-start.3 = (f32[3,128,128]{1,2,0:T(8,128)}, f32[3,128,128]{1,2,0:T(8,128)S(1)}, u32[]{:S(2)}) copy-start(f32[3,128,128]{1,2,0:T(8,128)S(1)} %get-tuple-element.321) | copy-start | bytes 589828 | tf_op jit(solution)/shard_map/while
  93.2 3.0 %copy-start.8 = (f32[16]{0:T(128)S(1)}, f32[16]{0:T(128)}, u32[]{:S(2)}) copy-start(f32[16]{0:T(128)} %copy-done.7) | copy-start | bytes 196 | tf_op jit(solution)/shard_map/while
  96.1 2.1 %copy-start.4 = (f32[3,128,128]{1,2,0:T(8,128)S(1)}, f32[3,128,128]{1,2,0:T(8,128)}, u32[]{:S(2)}) copy-start(f32[3,128,128]{1,2,0:T(8,128)} %copy-done.3) | copy-start | bytes 589828 | tf_op jit(solution)/shard_map/while
  98.3 2.1 %copy-start.3 = (f32[3,128,128]{1,2,0:T(8,128)}, f32[3,128,128]{1,2,0:T(8,128)S(1)}, u32[]{:S(2)}) copy-start(f32[3,128,128]{1,2,0:T(8,128)S(1)} %get-tuple-element.321) | copy-start | bytes 589828 | tf_op jit(solution)/shard_map/while
  105.4 3.0 %copy-start.8 = (f32[16]{0:T(128)S(1)}, f32[16]{0:T(128)}, u32[]{:S(2)}) copy-start(f32[16]{0:T(128)} %copy-done.7) | copy-start | bytes 196 | tf_op jit(solution)/shard_map/while
  108.4 2.1 %copy-start.4 = (f32[3,128,128]{1,2,0:T(8,128)S(1)}, f32[3,128,128]{1,2,0:T(8,128)}, u32[]{:S(2)}) copy-start(f32[3,128,128]{1,2,0:T(8,128)} %copy-done.3) | copy-start | bytes 589828 | tf_op jit(solution)/shard_map/while
  110.6 2.1 %copy-start.3 = (f32[3,128,128]{1,2,0:T(8,128)}, f32[3,128,128]{1,2,0:T(8,128)S(1)}, u32[]{:S(2)}) copy-start(f32[3,128,128]{1,2,0:T(8,128)S(1)} %get-tuple-element.321) | copy-start | bytes 589828 | tf_op jit(solution)/shard_map/while
  117.7 3.0 %copy-start.8 = (f32[16]{0:T(128)S(1)}, f32[16]{0:T(128)}, u32[]{:S(2)}) copy-start(f32[16]{0:T(128)} %copy-done.7) | copy-start | bytes 196 | tf_op jit(solution)/shard_map/while
  120.7 2.1 %copy-start.4 = (f32[3,128,128]{1,2,0:T(8,128)S(1)}, f32[3,128,128]{1,2,0:T(8,128)}, u32[]{:S(2)}) copy-start(f32[3,128,128]{1,2,0:T(8,128)} %copy-done.3) | copy-start | bytes 589828 | tf_op jit(solution)/shard_map/while
  145.1 50.6 %all-to-all-start.1 = ((bf16[512,8,80]{0,2,1:T(8,128)(2,1)}), bf16[512,8,80]{0,2,1:T(8,128)(2,1)S(1)}, u32[]{:S(2)}, u32[]{:S(2)}) async-start(bf16[512,8,80]{0,2,1:T(8,128)(2,1)} %bitcast.166), calls=%async_computation.2 | async-start | bytes 1310720 | tf_op jit(solution)/shard_map/all_to_all | solution.py:187
  183.3 8.3 %copy-start.20 = (f32[3,16,64,128]{3,2,1,0:T(8,128)S(1)}, f32[3,16,64,128]{3,2,1,0:T(8,128)}, u32[]{:S(2)}) copy-start(f32[3,16,64,128]{3,2,1,0:T(8,128)} %get-tuple-element.89) | copy-start | bytes 4718596
  (6 other events, 5.1 us)
Sparse Core Ops, SparseCore 0:
  36.7 26.0 all-gather.4
  85.8 33.8 reduce-scatter.1
Sparse Core Ops, SparseCore 1:
  123.7 59.5 all-gather.6
